TPU v7x, 512 devices: a whole 4x8x8 slice. The times are simulated.
512 devices in a mesh: sp: 32 (over z, x), tp: 16 (over y, core).
Axes of the slice: x: 4, y: 8, z: 8, core: 2. Of those that a mesh axis runs over, the one named last changes fastest.
Arguments:
- queries: bfloat16 [8192, 1536], P('sp', 'tp'), may hold values from -500 to 500
- latent: bfloat16 [8192, 256], P('sp'), may hold values from -6 to 6
- rope_key: bfloat16 [8192, 32], P('sp'), may hold values from -6 to 6
- latent_gain: bfloat16 [256], replicated, may hold values from 0.099609375 to 1.8984375
- key_value_weight: bfloat16 [256, 2048], P(None, 'tp'), may hold values from -0.375 to 0.375
- out_weight: bfloat16 [1024, 2048], P(None, 'tp'), may hold values from -6 to 6
- residual: bfloat16 [8192, 2048], P('sp', 'tp'), may hold values from -150 to 150
- ffn_gain: bfloat16 [2048], replicated, may hold values from 0.099609375 to 1.8984375
- routes: int32 [8192, 2], P('sp'), may hold values from 0 to 31, all different within a row; in each aligned block of 256 rows (0 to 255, 256 to 511, ...) at most 32 rows name the same one
- route_prob: float32 [8192, 2], P('sp'), may hold values from 0.1 to 1
- group_weight: float32 [8192], P('sp'), may hold values from 0.25 to 1
- gate_weight: bfloat16 [32, 2048, 4096], P('sp', None, 'tp'), may hold values from -0.125 to 0.125
- up_weight: bfloat16 [32, 2048, 4096], P('sp', None, 'tp'), may hold values from -0.125 to 0.125
- down_weight: bfloat16 [32, 4096, 2048], P('sp', None, 'tp'), may hold values from -0.75 to 0.75
Outputs:
- final: bfloat16 [8192, 2048], P('sp', 'tp')
Inputs may be any that keep to these rules, and one draw needn't show every extreme that they name: `routes`: each row names 2 different experts; among the 256 rows of one index of sp no expert is named more than 32 times, a bound that some block reaches.
All inputs are finite; a program needn't handle non-finite values.
Results may differ from a plain program's by a relative error of at most 0.015.
The roundings to bfloat16 on the way count: a program that leaves them out, or rounds other values in their place, can miss the bound.
Values may be sent and summed in bfloat16 or wider, within the bound.
No kernel may reach another device: no remote copies, remote signals or barrier semaphores. Data moves between devices by JAX's collectives and lax.ppermute only.
A program may use at most 64 MiB of HBM per device.

v0:
```python
import jax
import jax.numpy as jnp
from jax import lax
from jax.sharding import PartitionSpec as P

D = 2048
NOPE = 64
ROPE = 32
VDIM = 64
TOP = 2
SPAN = 64
EXP_DEV = 1
THETA = 500000.0
EPSILON = 1e-06


def rotate(values, positions):
    rot_width = values.shape[-1]
    half_width = rot_width // 2
    frequency = 1.0 / THETA ** (jnp.arange(0, rot_width, 2, dtype=jnp.float32) / rot_width)
    angles = positions.astype(jnp.float32)[:, None] * frequency[None, :]
    view_shape = (values.shape[0],) + (1,) * (values.ndim - 2) + (half_width,)
    cos_table = jnp.cos(angles).reshape(view_shape)
    sin_table = jnp.sin(angles).reshape(view_shape)
    wide = values.astype(jnp.float32)
    lower_half = wide[..., :half_width]
    upper_half = wide[..., half_width:]
    return jnp.concatenate(
        [
            lower_half * cos_table - upper_half * sin_table,
            upper_half * cos_table + lower_half * sin_table,
        ],
        axis=-1,
    )


def body(
    queries,
    latent,
    rope_key,
    latent_gain,
    key_value_weight,
    out_weight,
    residual,
    ffn_gain,
    routes,
    route_prob,
    group_weight,
    gate_weight,
    up_weight,
    down_weight,
):
    tokens_here = queries.shape[0]
    heads_here = key_value_weight.shape[1] // (NOPE + VDIM)
    width_here = residual.shape[1]
    offset = lax.axis_index("sp") * tokens_here
    positions = offset + jnp.arange(tokens_here, dtype=jnp.int32)
    query = queries.reshape(tokens_here, heads_here, NOPE + ROPE)
    query_nope = query[..., :NOPE]
    query_rope = rotate(query[..., NOPE:], positions).astype(jnp.bfloat16)
    query_blocks = positions // SPAN
    last_block = query_blocks[-1]
    scaling = (NOPE + ROPE) ** (-0.5)

    def attend(state_in, key_value, rotated):
        length = rotated.shape[0]
        running_max, normalizer, weighted = state_in
        key_value = key_value.reshape(length, heads_here, NOPE + VDIM)
        scores = jnp.einsum(
            "qhd,khd->qhk", query_nope, key_value[..., :NOPE], preferred_element_type=jnp.float32
        )
        scores = scores + jnp.einsum(
            "qhd,kd->qhk", query_rope, rotated, preferred_element_type=jnp.float32
        )
        scores = scores * scaling
        key_blocks = jnp.arange(length, dtype=jnp.int32) // SPAN
        allowed = key_blocks[None, :] <= query_blocks[:, None]
        scores = jnp.where(allowed[:, None, :], scores, -jnp.inf)
        new_max = jnp.maximum(running_max, jnp.max(scores, axis=-1))
        exp_scores = jnp.exp(scores - new_max[..., None])
        normalizer = jnp.sum(exp_scores, axis=-1)
        weighted = jnp.einsum(
            "qhk,khd->qhd",
            exp_scores.astype(jnp.bfloat16),
            key_value[..., NOPE:],
            preferred_element_type=jnp.float32,
        )
        return (new_max, normalizer, weighted)

    initial = (
        jnp.full((tokens_here, heads_here), -1e30, jnp.float32),
        jnp.zeros((tokens_here, heads_here), jnp.float32),
        jnp.zeros((tokens_here, heads_here, VDIM), jnp.float32),
    )
    length = latent.shape[0]
    latent_wide = latent.astype(jnp.float32)
    normed = latent_wide * lax.rsqrt(
        jnp.mean(latent_wide * latent_wide, axis=-1, keepdims=True) + EPSILON
    )
    normed = (normed * latent_gain.astype(jnp.float32)).astype(jnp.bfloat16)
    key_value = jnp.dot(normed, key_value_weight, preferred_element_type=jnp.float32).astype(
        jnp.bfloat16
    )
    rotated = rotate(rope_key, offset + jnp.arange(length, dtype=jnp.int32)).astype(jnp.bfloat16)
    pieces = (
        lax.all_gather(key_value, "sp", axis=0, tiled=True),
        lax.all_gather(rotated, "sp", axis=0, tiled=True),
    )

    def attend_piece(kept):
        return attend(kept, pieces[0], pieces[1])

    running_max, normalizer, weighted = lax.cond(
        jnp.int32(0) // SPAN > last_block, lambda kept: kept, attend_piece, initial
    )
    attended = (
        (weighted / normalizer[..., None])
        .astype(jnp.bfloat16)
        .reshape(tokens_here, heads_here * VDIM)
    )
    projected = jnp.dot(
        lax.all_gather(attended, "tp", axis=1, tiled=True),
        out_weight,
        preferred_element_type=jnp.float32,
    )
    mixed_rows = (residual.astype(jnp.float32) + projected).astype(jnp.bfloat16)
    mixed_wide = mixed_rows.astype(jnp.float32)
    sp_count = lax.axis_size("sp")
    experts_all = EXP_DEV * sp_count
    capacity = 2 * tokens_here * TOP // experts_all
    picks = routes.reshape(-1)
    onehot = (picks[:, None] == jnp.arange(experts_all, dtype=jnp.int32)[None, :]).astype(jnp.int32)
    slot_index = jnp.sum((jnp.cumsum(onehot, axis=0) - 1) * onehot, axis=1)
    target = picks * capacity + slot_index
    token_of = jnp.arange(tokens_here * TOP, dtype=jnp.int32) // TOP
    row_shape = (sp_count, EXP_DEV, capacity)

    def place(source_rows):
        empty = jnp.zeros((experts_all * capacity,) + source_rows.shape[1:], source_rows.dtype)
        filled = empty.at[target].set(source_rows[token_of])
        return filled.reshape((sp_count, EXP_DEV * capacity) + source_rows.shape[1:])

    row_squares = lax.psum(jnp.sum(mixed_wide * mixed_wide, axis=-1), "tp")
    row_scale = lax.rsqrt(row_squares / D + EPSILON)
    gain_here = lax.dynamic_slice_in_dim(
        ffn_gain, lax.axis_index("tp") * width_here, width_here, 0
    ).astype(jnp.float32)
    scaled = (mixed_wide * gain_here[None, :]).astype(jnp.bfloat16)
    arrived_rows, arrived_scale = (
        lax.all_to_all(place(scaled), "sp", split_axis=0, concat_axis=0, tiled=True),
        lax.all_to_all(
            place(row_scale).astype(jnp.bfloat16), "sp", split_axis=0, concat_axis=0, tiled=True
        ).astype(jnp.float32),
    )
    part_rows = lax.all_gather(arrived_rows, "tp", axis=2, tiled=True)
    inputs = part_rows.reshape(row_shape + (part_rows.shape[2],))
    length = inputs.shape[3]
    gate_acc = jnp.einsum("secd,edf->secf", inputs, gate_weight, preferred_element_type=jnp.float32)
    up_acc = jnp.einsum("secd,edf->secf", inputs, up_weight, preferred_element_type=jnp.float32)
    row_scales = arrived_scale.reshape(row_shape)
    gate_full = gate_acc * row_scales[..., None]
    up_full = up_acc * row_scales[..., None]
    hidden = (jax.nn.silu(gate_full) * up_full).astype(jnp.bfloat16)
    expert_out = jnp.einsum(
        "secf,efd->secd",
        lax.all_gather(hidden, "tp", axis=3, tiled=True),
        down_weight,
        preferred_element_type=jnp.float32,
    ).astype(jnp.bfloat16)
    returned_rows = lax.all_to_all(
        expert_out.reshape(sp_count, EXP_DEV * capacity, width_here),
        "sp",
        split_axis=0,
        concat_axis=0,
        tiled=True,
    )
    picked = (
        returned_rows.reshape(experts_all * capacity, width_here)[target]
        .astype(jnp.float32)
        .reshape(tokens_here, TOP, width_here)
    )
    combine = group_weight[:, None] * route_prob / jnp.sum(route_prob, axis=-1, keepdims=True)
    routed_sum = jnp.sum(combine[..., None] * picked, axis=1)
    return (mixed_wide + routed_sum).astype(jnp.bfloat16)


def solution(mesh):
    return jax.shard_map(
        body,
        mesh=mesh,
        in_specs=(
            P("sp", "tp"),
            P("sp", None),
            P("sp", None),
            P(),
            P(None, "tp"),
            P(None, "tp"),
            P("sp", "tp"),
            P(),
            P("sp", None),
            P("sp", None),
            P("sp"),
            P("sp", None, "tp"),
            P("sp", None, "tp"),
            P("sp", None, "tp"),
        ),
        out_specs=P("sp", "tp"),
        check_vma=False,
    )
```

profile of v0, /device:TPU:8, one launch (start us, length us, event | category | flops | bytes accessed | tf_op | source)
XLA Modules:
  0.0 303.7 jit_solution(12168150198286247200)
XLA Ops:
  8.3 1.8 convolution_convert_fusion
  14.2 1.2 reduce-window.6
  18.6 50.2 %all_gather.16 = bf16[8192,32]{0,1:T(8,128)(2,1)S(1)} all-gather(bf16[256,32]{0,1:T(8,128)(2,1)S(1)} %pad_maximum_fusion.1), channel_id=1, replica_groups=mesh['sp'=32,'tp'=16] {'sp'}, dimensions={0}, use_global_device_ids=true | all-gather | bytes 540672 | tf_op jit(solution)/shard_map/all_gather | solution.py:107
  68.7 30.5 %all-gather.5.cloned.1.call-done = bf16[8192,128]{1,0:T(8,128)(2,1)} async-done(((bf16[256,128]{1,0:T(8,128)(2,1)}), bf16[8192,128]{1,0:T(8,128)(2,1)}) %all-gather.5.cloned.1.call-update) | async-done | bytes 2097168 | tf_op jit(solution)/shard_map/all_gather | solution.py:106
  99.3 6.8 %conditional.1 = (f32[256,1]{0,1:T(1,128)S(1)}, f32[256,1,64]{0,2,1:T(8,128)S(1)}) conditional(s32[]{:T(128)} %bitcast.13, (s32[256]{0:T(256)S(1)}, bf16[8192,128]{1,0:T(8,128)(2,1)}, bf16[256,1,96]{0,2,1:T(8,128)(2,1)}, bf16[256,1,32]{0,2,1:T(8,128)(2,1)S(1)}, bf16[8192,32]{0,1:T(8,128)(2,1)S(1)}) %tuple.30, () %tuple.14), branch_computations={%region_1.4_spmd, %region_4.5_spmd} | conditional | flops 690028288 | bytes 55434312 | solution.py:113
  99.3 1.3 convolution_bitcast_fusion
  100.9 1.9 fusion.67
  102.9 2.0 fusion.9
  104.9 1.2 fusion.4
  106.1 17.3 %all-gather = bf16[256,1,1024]{0,2,1:T(8,128)(2,1)S(1)} all-gather(bf16[256,1,64]{0,2,1:T(8,128)(2,1)S(1)} %divide_convert_fusion), channel_id=2, replica_groups=mesh['sp'=32,'tp'=16] {'tp'}, dimensions={2}, use_global_device_ids=true | all-gather | bytes 557056 | tf_op jit(solution)/shard_map/all_gather | solution.py:122
  123.7 3.1 %scatter_custom_fusion = bf16[1024,128]{1,0:T(8,128)(2,1)S(1)} fusion(s32[512]{0:T(512)S(1)} %bitcast.133, bf16[256,128]{1,0:T(8,128)(2,1)S(1)} %copy.51, s32[1024]{0:T(1024)S(1)} %pad_clamp_fusion.1, bf16[]{:T(256)} %constant.117.clone.1), kind=kCustom, calls=%fused_computation.56 | custom fusion | bytes 262146 | tf_op jit(solution)/shard_map/scatter | solution.py:140
  126.8 18.9 %all_to_all.16 = bf16[32,32,128]{2,1,0:T(8,128)(2,1)} all-to-all(bf16[32,32,128]{2,1,0:T(8,128)(2,1)S(1)} %bitcast.127), channel_id=1, replica_groups=mesh['sp'=32,'tp'=16] {'sp'}, dimensions={0} | all-to-all | bytes 524288 | tf_op jit(solution)/shard_map/all_to_all | solution.py:150
  145.8 22.2 %psum.7 = f32[256]{0:T(256)S(1)} all-reduce(f32[256]{0:T(256)S(1)} %get-tuple-element.37), channel_id=1, replica_groups=mesh['sp'=32,'tp'=16] {'tp'}, use_global_device_ids=true, to_apply=%region_11.12 | all-reduce | flops 256 | bytes 2048 | tf_op jit(solution)/shard_map/psum | solution.py:143
  167.9 3.5 %gather_fusion = f32[512]{0:T(512)S(1)} fusion(f32[256]{0:T(256)S(1)} %add_rsqrt_fusion, s32[1024]{0:T(1024)S(1)} %pad_clamp_fusion.1), kind=kCustom, calls=%fused_computation.1 | custom fusion | bytes 6144 | tf_op jit(solution)/shard_map/gather | solution.py:140
  171.5 2.4 scatter_custom_fusion.1
  174.0 13.8 %all_to_all.17 = bf16[32,1,32]{2,1,0:T(2,128)(2,1)S(1)} all-to-all(bf16[32,1,32]{2,1,0:T(2,128)(2,1)S(1)} %convert_element_type.138), channel_id=1, replica_groups=mesh['sp'=32,'tp'=16] {'sp'}, dimensions={0} | all-to-all | bytes 4096 | tf_op jit(solution)/shard_map/all_to_all | solution.py:151
  187.8 3.1 %all-gather.7.cloned.1.call-done = bf16[32,32,2048]{2,1,0:T(8,128)(2,1)} async-done(((bf16[32,32,128]{2,1,0:T(8,128)(2,1)}), bf16[32,32,2048]{2,1,0:T(8,128)(2,1)}) %all-gather.7.cloned.1.call-update) | async-done | bytes 4194320 | tf_op jit(solution)/shard_map/all_gather | solution.py:155
  190.9 3.5 %fusion.23 = f32[32,1,32,256]{3,2,0,1:T(8,128)S(1)} fusion(bf16[32,32,2048]{2,1,0:T(8,128)(2,1)} %all-gather.7.cloned.1.call-done, bf16[1,2048,256]{2,1,0:T(8,128)(2,1)S(1)} %copy-done, f32[32,32]{1,0:T(8,128)S(1)} %bitcast.131), kind=kOutput, calls=%fused_computation.37 | convolution fusion | flops 1074003968 | bytes 6295552 | tf_op jit(solution)/shard_map/secd,edf->secf/dot_general | solution.py:158
  194.4 4.4 %fusion.25 = bf16[32,1,32,256]{3,2,0,1:T(8,128)(2,1)} fusion(bf16[32,32,2048]{2,1,0:T(8,128)(2,1)} %all-gather.7.cloned.1.call-done, bf16[1,2048,256]{2,1,0:T(8,128)(2,1)S(1)} %copy-done.6, f32[32,1,32,256]{3,2,0,1:T(8,128)S(1)} %fusion.23, f32[32,32]{1,0:T(8,128)S(1)} %bitcast.132), kind=kOutput, calls=%fused_computation.39 | convolution fusion | flops 1075576832 | bytes 6819840 | tf_op jit(solution)/shard_map/secd,edf->secf/dot_general | solution.py:159
  198.8 66.5 %all-gather.9.cloned.1.call-done = bf16[32,1,32,4096]{3,2,0,1:T(8,128)(2,1)} async-done(((bf16[32,1,32,256]{3,2,0,1:T(8,128)(2,1)}), bf16[32,1,32,4096]{3,2,0,1:T(8,128)(2,1)}) %all-gather.9.cloned.1.call-update) | async-done | bytes 8388624 | tf_op jit(solution)/shard_map/all_gather | solution.py:166
  265.3 6.4 %fusion.26 = bf16[32,32,128]{2,1,0:T(8,128)(2,1)} fusion(bf16[32,1,32,4096]{3,2,0,1:T(8,128)(2,1)} %all-gather.9.cloned.1.call-done, bf16[1,4096,128]{2,1,0:T(8,128)(2,1)S(1)} %copy-done.7), kind=kOutput, calls=%fused_computation.40 | convolution fusion | flops 1073872896 | bytes 9699328 | tf_op jit(solution)/shard_map/secf,efd->secd/dot_general | solution.py:164
  271.8 9.4 %all-to-all-start.2 = ((bf16[32,32,128]{2,1,0:T(8,128)(2,1)}), bf16[32,32,128]{2,1,0:T(8,128)(2,1)S(1)}, u32[]{:S(2)}, u32[]{:S(2)}) async-start(bf16[32,32,128]{2,1,0:T(8,128)(2,1)} %fusion.26), calls=%async_computation.2 | async-start | bytes 524288 | tf_op jit(solution)/shard_map/all_to_all | solution.py:170
  281.4 13.2 %all-to-all-done.2 = bf16[32,32,128]{2,1,0:T(8,128)(2,1)S(1)} async-done(((bf16[32,32,128]{2,1,0:T(8,128)(2,1)}), bf16[32,32,128]{2,1,0:T(8,128)(2,1)S(1)}, u32[]{:S(2)}, u32[]{:S(2)}) %all-to-all-start.2) | async-done | bytes 262176 | tf_op jit(solution)/shard_map/all_to_all | solution.py:170
  294.6 1.3 gather_fusion.1
  (68 shorter events, 10.7 us)
Async XLA Ops:
  6.5 184.4 %copy-start = (bf16[1,2048,256]{2,1,0:T(8,128)(2,1)S(1)}, bf16[1,2048,256]{2,1,0:T(8,128)(2,1)}, u32[]{:S(2)}) copy-start(bf16[1,2048,256]{2,1,0:T(8,128)(2,1)} %param.27) | copy-start | bytes 3145732
  6.5 92.7 %all-gather.5.cloned.1.call-start = ((), (), s32[]{:S(2)}) async-start(), calls=%async_computation.3 | async-start | bytes 2162688 | tf_op jit(solution)/shard_map/all_gather | solution.py:106
  10.1 180.8 %all-gather.7.cloned.1.call-start = ((), (), s32[]{:S(2)}) async-start(), calls=%async_computation.4 | async-start | bytes 4456448 | tf_op jit(solution)/shard_map/all_gather | solution.py:155
  99.3 24.1 %copy-start.2 = (bf16[1024,128]{1,0:T(8,128)(2,1)S(1)}, bf16[1024,128]{1,0:T(8,128)(2,1)}, u32[]{:S(2)}) copy-start(bf16[1024,128]{1,0:T(8,128)(2,1)} %param.21) | copy-start | bytes 786436
  99.3 1.6 copy-start.1
  99.3 1.6 copy-start.3
  106.0 88.4 %copy-start.6 = (bf16[1,2048,256]{2,1,0:T(8,128)(2,1)S(1)}, bf16[1,2048,256]{2,1,0:T(8,128)(2,1)}, u32[]{:S(2)}) copy-start(bf16[1,2048,256]{2,1,0:T(8,128)(2,1)} %param.28) | copy-start | bytes 3145732
  145.7 119.6 %all-gather.9.cloned.1.call-start = ((), (), s32[]{:S(2)}) async-start(), calls=%async_computation.5 | async-start | bytes 8912896 | tf_op jit(solution)/shard_map/all_gather | solution.py:166
  190.9 74.5 %copy-start.7 = (bf16[1,4096,128]{2,1,0:T(8,128)(2,1)S(1)}, bf16[1,4096,128]{2,1,0:T(8,128)(2,1)}, u32[]{:S(2)}) copy-start(bf16[1,4096,128]{2,1,0:T(8,128)(2,1)} %param.29) | copy-start | bytes 3145732
  198.8 82.4 %copy-start.4 = (f32[256,2]{0,1:T(2,128)S(1)}, f32[256,2]{0,1:T(2,128)}, u32[]{:S(2)}) copy-start(f32[256,2]{0,1:T(2,128)} %param.25) | copy-start | bytes 6148
  198.8 82.4 %copy-start.5 = (f32[256]{0:T(256)S(1)}, f32[256]{0:T(256)}, u32[]{:S(2)}) copy-start(f32[256]{0:T(256)} %param.26) | copy-start | bytes 3076
  271.8 22.8 %all-to-all-start.2 = ((bf16[32,32,128]{2,1,0:T(8,128)(2,1)}), bf16[32,32,128]{2,1,0:T(8,128)(2,1)S(1)}, u32[]{:S(2)}, u32[]{:S(2)}) async-start(bf16[32,32,128]{2,1,0:T(8,128)(2,1)} %fusion.26), calls=%async_computation.2 | async-start | bytes 524288 | tf_op jit(solution)/shard_map/all_to_all | solution.py:170
Sparse Core Ops, SparseCore 0:
  10.5 88.7 all-gather.4
  145.8 45.0 all-gather.6
  199.0 66.3 all-gather.8
where the time goes:
time: 304 us
  blocking collectives  122 us (40%)
  waiting for transfers between devices  113 us (37%)
  matrix products  21.6 us (7%)
  local copies, waits for them, and re-layouts  15 us (5%)
  between operations  14 us (5%)
  starting transfers between devices  9.5 us (3%)
  other arithmetic  8.01 us (3%)
    all_gather x1, waiting for transfers between devices, body(): lax.all_gather(hidden, 'tp', axis=3, tiled=True)  66.5 us
    all_gather x1, blocking collectives, body(): lax.all_gather(rotated, 'sp', axis=0, tiled=True)  50.2 us
    all_gather x1, waiting for transfers between devices, body(): lax.all_gather(key_value, 'sp', axis=0, tiled=True)  30.5 us
    psum x1, blocking collectives, body(): row_squares = lax.psum(jnp.sum(mixed_wide * mixed_wide, axis=-1), 'tp')  22.2 us
    all_to_all x1, blocking collectives, body(): lax.all_to_all(place(scaled), 'sp', split_axis=0, concat_axis=0, tiled=True)  18.9 us
    all_gather x1, blocking collectives, body(): lax.all_gather(attended, 'tp', axis=1, tiled=True)  17.3 us
    all_to_all x1, blocking collectives, body(): lax.all_to_all(place(row_scale).astype(jnp.bfloat16), 'sp', split_axis=0,...  13.8 us
    all_to_all x1, waiting for transfers between devices, body(): lax.all_to_all(expert_out.reshape(sp_count, EXP_DEV * capacity, width_her...  13.2 us
  transfers between devices with their start and end apart: 4, of which 4 were waited for; matrix products, arithmetic and copies ran while one was open for 5% of the time, Pallas kernels for 0%

commit v1 on v0

--- a/solution.py
+++ b/solution.py
@@ -163,7 +163,9 @@
     hidden = (jax.nn.silu(gate_full) * up_full).astype(jnp.bfloat16)
     expert_out = jnp.einsum(
         "secf,efd->secd",
-        lax.all_gather(hidden, "tp", axis=3, tiled=True),
+        jnp.concatenate(
+            lax.all_to_all(jnp.stack([hidden] * lax.axis_size("tp")), "tp", 0, 0), axis=3
+        ),
         down_weight,
         preferred_element_type=jnp.float32,
     ).astype(jnp.bfloat16)

time: 304 us -> 460 us (1.51)
  the two profiles are of different devices: /device:TPU:8 before, /device:TPU:1 now
where the time goes in v1:
time: 460 us; the launch traced here: 458 us
  blocking collectives  312 us (68%)
  waiting for transfers between devices  49 us (11%)
  local copies, waits for them, and re-layouts  44.7 us (10%)
  matrix products  20.7 us (4%)
  between operations  14.3 us (3%)
  starting transfers between devices  9.84 us (2%)
  other arithmetic  8 us (2%)
    all_to_all x1, blocking collectives, body(): lax.all_to_all(jnp.stack([hidden] * lax.axis_size('tp')), 'tp', 0, 0)  189 us
    all_gather x1, blocking collectives, body(): lax.all_gather(rotated, 'sp', axis=0, tiled=True)  43.7 us
    all_gather x1, waiting for transfers between devices, body(): lax.all_gather(key_value, 'sp', axis=0, tiled=True)  33 us
    psum x1, blocking collectives, body(): row_squares = lax.psum(jnp.sum(mixed_wide * mixed_wide, axis=-1), 'tp')  25.5 us
    all_gather x1, blocking collectives, body(): lax.all_gather(attended, 'tp', axis=1, tiled=True)  24 us
    all_to_all x1, blocking collectives, body(): lax.all_to_all(place(scaled), 'sp', split_axis=0, concat_axis=0, tiled=True)  16.7 us
    reshape x1, local copies, waits for them, and re-layouts, body(): jnp.concatenate(lax.all_to_all(jnp.stack([hidden] * lax.axis_size('tp')),...  15.1 us
    another operation x2, local copies, waits for them, and re-layouts  13.6 us
  transfers between devices with their start and end apart: 3, of which 3 were waited for; matrix products, arithmetic and copies ran while one was open for 3% of the time, Pallas kernels for 0%

profile of v1, /device:TPU:1, one launch (start us, length us, event | category | flops | bytes accessed | tf_op | source)
XLA Modules:
  0.0 458.4 jit_solution(314667414025123197)
XLA Ops:
  8.3 1.8 convolution_convert_fusion.1
  18.5 43.7 %all_gather.13 = bf16[8192,32]{0,1:T(8,128)(2,1)S(1)} all-gather(bf16[256,32]{0,1:T(8,128)(2,1)S(1)} %pad_maximum_fusion.1), channel_id=1, replica_groups=mesh['sp'=32,'tp'=16] {'sp'}, dimensions={0}, use_global_device_ids=true | all-gather | bytes 540672 | tf_op jit(solution)/shard_map/all_gather | solution.py:107
  62.2 33.0 %all-gather.4.cloned.1.call-done = bf16[8192,128]{1,0:T(8,128)(2,1)} async-done(((bf16[256,128]{1,0:T(8,128)(2,1)}), bf16[8192,128]{1,0:T(8,128)(2,1)}) %all-gather.4.cloned.1.call-update) | async-done | bytes 2097168 | tf_op jit(solution)/shard_map/all_gather | solution.py:106
  95.2 6.8 %conditional.1 = (f32[256,1]{0,1:T(1,128)S(1)}, f32[256,1,64]{0,2,1:T(8,128)S(1)}) conditional(s32[]{:T(128)} %bitcast.13, (s32[256]{0:T(256)S(1)}, bf16[8192,128]{1,0:T(8,128)(2,1)}, bf16[256,1,96]{0,2,1:T(8,128)(2,1)}, bf16[256,1,32]{0,2,1:T(8,128)(2,1)S(1)}, bf16[8192,32]{0,1:T(8,128)(2,1)S(1)}) %tuple.28, () %tuple.14), branch_computations={%region_1.4_spmd, %region_4.5_spmd} | conditional | flops 690028288 | bytes 55434312 | solution.py:113
  95.2 1.3 convolution_bitcast_fusion
  96.9 2.0 fusion.63
  100.0 2.0 fusion.9
  102.0 24.0 %all-gather = bf16[256,1,1024]{0,2,1:T(8,128)(2,1)S(1)} all-gather(bf16[256,1,64]{0,2,1:T(8,128)(2,1)S(1)} %divide_convert_fusion), channel_id=2, replica_groups=mesh['sp'=32,'tp'=16] {'tp'}, dimensions={2}, use_global_device_ids=true | all-gather | bytes 557056 | tf_op jit(solution)/shard_map/all_gather | solution.py:122
  126.4 3.1 scatter_custom_fusion
  129.5 16.7 %all_to_all.21 = bf16[32,32,128]{2,1,0:T(8,128)(2,1)} all-to-all(bf16[32,32,128]{2,1,0:T(8,128)(2,1)S(1)} %bitcast.135), channel_id=1, replica_groups=mesh['sp'=32,'tp'=16] {'sp'}, dimensions={0} | all-to-all | bytes 524288 | tf_op jit(solution)/shard_map/all_to_all | solution.py:150
  146.2 25.5 %psum.7 = f32[256]{0:T(256)S(1)} all-reduce(f32[256]{0:T(256)S(1)} %get-tuple-element.37), channel_id=1, replica_groups=mesh['sp'=32,'tp'=16] {'tp'}, use_global_device_ids=true, to_apply=%region_11.12 | all-reduce | flops 256 | bytes 2048 | tf_op jit(solution)/shard_map/psum | solution.py:143
  171.7 3.5 gather_fusion
  175.2 2.4 scatter_custom_fusion.1
  177.8 12.5 %all_to_all.22 = bf16[32,1,32]{2,1,0:T(2,128)(2,1)S(1)} all-to-all(bf16[32,1,32]{2,1,0:T(2,128)(2,1)S(1)} %convert_element_type.141), channel_id=1, replica_groups=mesh['sp'=32,'tp'=16] {'sp'}, dimensions={0} | all-to-all | bytes 4096 | tf_op jit(solution)/shard_map/all_to_all | solution.py:151
  190.3 3.4 all-gather.6.cloned.1.call-done
  193.8 3.4 fusion.21
  197.2 3.5 fusion.24
  201.8 189.5 %all_to_all.23 = bf16[16,32,1,32,256]{4,3,1,2,0:T(8,128)(2,1)} all-to-all(bf16[16,32,1,32,256]{4,3,1,2,0:T(8,128)(2,1)S(1)} %stack.2), channel_id=1, replica_groups=mesh['sp'=32,'tp'=16] {'tp'}, dimensions={0} | all-to-all | bytes 16777216 | tf_op jit(solution)/shard_map/all_to_all | solution.py:167
  391.3 15.1 %copy.54 = bf16[32,1,32,16,256]{4,3,2,0,1:T(8,128)(2,1)} copy(bf16[32,1,32,16,256]{4,2,0,1,3:T(8,128)(2,1)} %bitcast.131) | data formatting | bytes 16777216 | tf_op jit(solution)/shard_map/reshape | solution.py:166
  406.4 13.6 %reshape.392 = bf16[32,32,4096]{2,1,0:T(8,128)(2,1)} reshape(bf16[32,1,32,16,256]{4,3,2,0,1:T(8,128)(2,1)} %copy.54) | data formatting | bytes 16777216 | tf_op jit(solution)/shard_map/reshape.37
  420.0 6.4 %convolution_convert_fusion = bf16[32,32,128]{2,1,0:T(8,128)(2,1)} fusion(bf16[32,32,4096]{2,1,0:T(8,128)(2,1)} %reshape.392, bf16[1,4096,128]{2,1,0:T(8,128)(2,1)S(1)} %copy-done.7), kind=kOutput, calls=%fused_computation.39 | convolution fusion | flops 1073872896 | bytes 9699328 | tf_op jit(solution)/shard_map/secf,efd->secd/dot_general | solution.py:164
  426.4 9.8 %all-to-all-start.3 = ((bf16[32,32,128]{2,1,0:T(8,128)(2,1)}), bf16[32,32,128]{2,1,0:T(8,128)(2,1)S(1)}, u32[]{:S(2)}, u32[]{:S(2)}) async-start(bf16[32,32,128]{2,1,0:T(8,128)(2,1)} %convolution_convert_fusion), calls=%async_computation.3 | async-start | bytes 524288 | tf_op jit(solution)/shard_map/all_to_all | solution.py:172
  436.4 12.5 %all-to-all-done.3 = bf16[32,32,128]{2,1,0:T(8,128)(2,1)S(1)} async-done(((bf16[32,32,128]{2,1,0:T(8,128)(2,1)}), bf16[32,32,128]{2,1,0:T(8,128)(2,1)S(1)}, u32[]{:S(2)}, u32[]{:S(2)}) %all-to-all-start.3) | async-done | bytes 262176 | tf_op jit(solution)/shard_map/all_to_all | solution.py:172
  449.0 1.3 gather_fusion.1
  (69 shorter events, 14.1 us)
Async XLA Ops:
  6.5 187.2 %copy-start = (bf16[1,2048,256]{2,1,0:T(8,128)(2,1)S(1)}, bf16[1,2048,256]{2,1,0:T(8,128)(2,1)}, u32[]{:S(2)}) copy-start(bf16[1,2048,256]{2,1,0:T(8,128)(2,1)} %param.27) | copy-start | bytes 3145732
  6.5 88.7 %all-gather.4.cloned.1.call-start = ((), (), s32[]{:S(2)}) async-start(), calls=%async_computation.4 | async-start | bytes 2162688 | tf_op jit(solution)/shard_map/all_gather | solution.py:106
  10.1 183.7 %all-gather.6.cloned.1.call-start = ((), (), s32[]{:S(2)}) async-start(), calls=%async_computation.5 | async-start | bytes 4456448 | tf_op jit(solution)/shard_map/all_gather | solution.py:155
  95.2 30.8 %copy-start.2 = (bf16[1024,128]{1,0:T(8,128)(2,1)S(1)}, bf16[1024,128]{1,0:T(8,128)(2,1)}, u32[]{:S(2)}) copy-start(bf16[1024,128]{1,0:T(8,128)(2,1)} %param.21) | copy-start | bytes 786436
  95.2 1.6 copy-start.1
  95.2 1.6 copy-start.3
  102.0 95.2 %copy-start.6 = (bf16[1,2048,256]{2,1,0:T(8,128)(2,1)S(1)}, bf16[1,2048,256]{2,1,0:T(8,128)(2,1)}, u32[]{:S(2)}) copy-start(bf16[1,2048,256]{2,1,0:T(8,128)(2,1)} %param.28) | copy-start | bytes 3145732
  406.4 13.6 %copy-start.7 = (bf16[1,4096,128]{2,1,0:T(8,128)(2,1)S(1)}, bf16[1,4096,128]{2,1,0:T(8,128)(2,1)}, u32[]{:S(2)}) copy-start(bf16[1,4096,128]{2,1,0:T(8,128)(2,1)} %param.29) | copy-start | bytes 3145732
  420.0 16.2 %copy-start.4 = (f32[256,2]{0,1:T(2,128)S(1)}, f32[256,2]{0,1:T(2,128)}, u32[]{:S(2)}) copy-start(f32[256,2]{0,1:T(2,128)} %param.25) | copy-start | bytes 6148
  420.0 16.3 %copy-start.5 = (f32[256]{0:T(256)S(1)}, f32[256]{0:T(256)}, u32[]{:S(2)}) copy-start(f32[256]{0:T(256)} %param.26) | copy-start | bytes 3076
  426.4 22.5 %all-to-all-start.3 = ((bf16[32,32,128]{2,1,0:T(8,128)(2,1)}), bf16[32,32,128]{2,1,0:T(8,128)(2,1)S(1)}, u32[]{:S(2)}, u32[]{:S(2)}) async-start(bf16[32,32,128]{2,1,0:T(8,128)(2,1)} %convolution_convert_fusion), calls=%async_computation.3 | async-start | bytes 524288 | tf_op jit(solution)/shard_map/all_to_all | solution.py:172
Sparse Core Ops, SparseCore 0:
  10.5 84.6 all-gather.3
  146.3 47.3 all-gather.5
